TPU v7x, 32 devices: a whole 2x2x4 slice. The times are simulated.
32 devices in a mesh: sp: 8 (over z, x), tp: 4 (over y, core).
Axes of the slice: x: 2, y: 2, z: 4, core: 2. Of those that a mesh axis runs over, the one named last changes fastest.
Arguments:
- query_one: bfloat16 [1024, 1024], P('sp', 'tp'), may hold values from -100 to 100
- key_one: bfloat16 [1024, 512], P('sp', 'tp'), may hold values from -10 to 10
- query_two: bfloat16 [1024, 1024], P('sp', 'tp'), may hold values from -100 to 100
- key_two: bfloat16 [1024, 512], P('sp', 'tp'), may hold values from -10 to 10
- value: bfloat16 [1024, 1024], P('sp', 'tp'), may hold values from -6 to 6
- lambda_head: float32 [8], P('tp'), may hold values from 0.3 to 0.8
- head_gain: float32 [256], replicated, may hold values from 0.1 to 1.9
- out_weight: bfloat16 [2048, 4096], P('tp'), may hold values from -0.125 to 0.125
- residual: bfloat16 [1024, 4096], P(('sp', 'tp')), may hold values from -6 to 6
- norm_gain: float32 [4096], replicated, may hold values from 0.1 to 1.9
- route_expert: int32 [1024, 2], P(('sp', 'tp')), may hold values from 0 to 7, all different within a row; in each aligned block of 32 rows (0 to 31, 32 to 63, ...) at most 16 rows name the same one
- route_weight: float32 [1024, 2], P(('sp', 'tp')), may hold values from 0.1 to 0.9
- expert_gate: bfloat16 [8, 4096, 1024], P('sp', None, 'tp'), may hold values from -0.09375 to 0.09375
- expert_up: bfloat16 [8, 4096, 1024], P('sp', None, 'tp'), may hold values from -0.09375 to 0.09375
- expert_down: bfloat16 [8, 1024, 4096], P('sp', 'tp'), may hold values from -0.1875 to 0.1875
Outputs:
- output: bfloat16 [1024, 4096], P(('sp', 'tp'))
Inputs may be any that keep to these rules, and one draw needn't show every extreme that they name: `route_expert`: the 2 entries of a row differ. In each aligned block of 32 rows (the rows of one device) no expert is named more than 16 times, a bound that some block reaches.
All inputs are finite; a program needn't handle non-finite values.
Results may differ from a plain program's by a relative error of at most 0.015.
Values may be sent and summed in bfloat16 or wider, within the bound.
A program may use at most 128 MiB of HBM per device.

v0:
```python
import functools
import math

import jax
import jax.numpy as jnp
from jax import lax
from jax.experimental import pallas as pl
from jax.experimental.pallas import tpu as pltpu
from jax.sharding import PartitionSpec as P

HEAD = 128
VMEM_BYTES = 58 * 1024 * 1024


def map_step(carried, query_rows, key_block, value_block, allowed):
    largest, totals, running = carried
    scores = jnp.einsum(
        "qcgd,kcd->cgqk", query_rows, key_block, preferred_element_type=jnp.float32
    ) * HEAD ** (-0.5)
    scores = jnp.where(allowed[None, None], scores, -jnp.inf)
    updated = jnp.maximum(largest, jnp.max(scores, axis=-1))
    weights = jnp.exp(scores - updated[..., None])
    rescale = jnp.exp(largest - updated)
    totals = totals * rescale + jnp.sum(weights, axis=-1)
    added = jnp.einsum(
        "cgqk,kce->qcge",
        weights.astype(jnp.bfloat16),
        value_block,
        preferred_element_type=jnp.float32,
    )
    running = running * jnp.transpose(rescale, (2, 0, 1))[..., None] + added
    return (updated, totals, running)


def finish(carried):
    return carried[2] / jnp.transpose(carried[1], (2, 0, 1))[..., None]


def remote(src, dst, send, recv, sp_to, tp_to):
    return pltpu.make_async_remote_copy(
        src_ref=src,
        dst_ref=dst,
        send_sem=send,
        recv_sem=recv,
        device_id={"sp": sp_to, "tp": tp_to},
        device_id_type=pl.DeviceIdType.MESH,
    )


def greet(peers):
    barrier = pltpu.get_barrier_semaphore()
    for sp_to, tp_to in peers:
        pl.semaphore_signal(
            barrier,
            inc=1,
            device_id={"sp": sp_to, "tp": tp_to},
            device_id_type=pl.DeviceIdType.MESH,
        )
    pl.semaphore_wait(barrier, len(peers))


def tp_place(tp):
    t = lax.axis_index("tp")
    c = lax.rem(t, 2)
    y = lax.div(t, 2)
    return t, y, c, 1 - c


def layer_kernel(
    sp, tp, heads, kv_heads, cap, span,
    q1, k1, q2, k2, v, lam, gain, ow_hbm, res, ngain, route_e, route_w,
    gate_hbm, up_hbm, down_hbm, out,
    kv, ow, att, pbuf, prc, pcs, pry, total, normed, placed, mix,
    gate, up, down, outg, tok, part, rc, cs, ry, fin, ret,
    ow_sem, z_send, z_recv, x_send, x_recv, pc_send, pc_recv, py_send, py_recv,
    w_sem, a_send, a_recv, y_send, y_recv, c_send, c_recv,
    rc_send, rc_recv, ry_send, ry_recv, ra_send, ra_recv,
):
    s = lax.axis_index("sp")
    t, y, c, pc = tp_place(tp)
    outer = tp // 2
    lanes = sp // 2
    px = s + 1 - 2 * lax.rem(s, 2)
    local = q1.shape[0]
    rows, width = out.shape
    tile = math.gcd(width, 512)
    core = y * 2 + pc
    kw = kv_heads * HEAD
    fetch = pltpu.make_async_copy(ow_hbm, ow, ow_sem)
    fetch.start()
    fetches = [
        pltpu.make_async_copy(gate_hbm, gate, w_sem.at[0]),
        pltpu.make_async_copy(up_hbm, up, w_sem.at[1]),
        pltpu.make_async_copy(down_hbm, down, w_sem.at[2]),
    ]
    for copy in fetches:
        copy.start()
    kv[s, :, 0:kw] = k1[...]
    kv[s, :, kw:2 * kw] = k2[...]
    kv[s, :, 2 * kw:4 * kw] = v[...]
    peers = [(lax.rem(s + k, sp), t) for k in range(1, sp)] + [(s, core)]
    peers += [(s, lax.rem(y + dy, outer) * 2 + c) for dy in range(1, outer)]
    greet(peers)
    sends = []
    for m in range(1, lanes):
        copy = remote(
            kv.at[s], kv.at[s], z_send.at[m], z_recv.at[m], lax.rem(s + 2 * m, sp), t
        )
        copy.start()
        sends.append(copy)

    def across(m):
        block = lax.rem(s + sp - 2 * m, sp)
        return remote(kv.at[block], kv.at[block], x_send.at[m], x_recv.at[m], px, t)

    places = lax.broadcasted_iota(jnp.int32, (rows, sp * cap), 1).astype(jnp.float32)
    owner = jnp.floor((places + 0.5) / cap)
    slot = places - owner * cap
    named = jnp.zeros((rows, sp * cap), jnp.float32)
    share = jnp.zeros((rows, sp * cap), jnp.float32)
    for choice in range(route_e.shape[1]):
        match = route_e[:, choice:choice + 1].astype(jnp.float32) == owner
        named += jnp.where(match, 1.0, 0.0)
        share += jnp.where(match, route_w[:, choice:choice + 1], 0.0)
    earlier = lax.broadcasted_iota(jnp.int32, (rows, rows), 1) < lax.broadcasted_iota(
        jnp.int32, (rows, rows), 0
    )
    rank = jnp.dot(
        jnp.where(earlier, 1.0, 0.0).astype(jnp.bfloat16),
        named.astype(jnp.bfloat16),
        preferred_element_type=jnp.float32,
    )
    held = jnp.where(rank == slot, named, 0.0)
    placed[...] = held.astype(jnp.bfloat16)
    mix[...] = share * held

    for m in range(lanes):
        if m:
            block = lax.rem(s + sp - 2 * m, sp)
            remote(kv.at[block], kv.at[block], z_send.at[m], z_recv.at[m], px, t).wait_recv()
        copy = across(m)
        copy.start()
        sends.append(copy)
    for m in range(lanes):
        block = lax.rem(px + sp - 2 * m, sp)
        remote(kv.at[block], kv.at[block], x_send.at[m], x_recv.at[m], px, t).wait_recv()

    length = sp * local
    key_pos = lax.broadcasted_iota(jnp.int32, (local, length), 1)
    query_pos = s * local + lax.broadcasted_iota(jnp.int32, (local, length), 0)
    allowed = key_pos <= query_pos
    per_key = heads // kv_heads
    for h in range(heads):
        g = h // per_key
        values = kv[:, :, 2 * kw + g * 2 * HEAD:2 * kw + (g + 1) * 2 * HEAD]
        values = values.reshape(length, 2 * HEAD)
        maps = []
        for which, q in ((0, q1), (1, q2)):
            start = which * kw + g * HEAD
            keys = kv[:, :, start:start + HEAD].reshape(length, HEAD)
            scores = lax.dot_general(
                q[:, h * HEAD:(h + 1) * HEAD],
                keys,
                (((1,), (1,)), ((), ())),
                preferred_element_type=jnp.float32,
            ) * HEAD ** (-0.5)
            scores = jnp.where(allowed, scores, -1e30)
            weights = jnp.exp(scores - jnp.max(scores, axis=-1, keepdims=True))
            totals = jnp.sum(weights, axis=-1, keepdims=True)
            added = jnp.dot(
                weights.astype(jnp.bfloat16), values, preferred_element_type=jnp.float32
            )
            maps.append(added / totals)
        difference = maps[0] - lam[h] * maps[1]
        scaled = (
            difference
            * lax.rsqrt(jnp.mean(difference * difference, axis=-1, keepdims=True) + 1e-05)
            * gain[...]
        )
        att[:, h * 2 * HEAD:(h + 1) * 2 * HEAD] = scaled.astype(jnp.bfloat16)

    fetch.wait()

    def begin(copy):
        copy.start()
        sends.append(copy)

    def share_pair(dy, p):
        group = lax.rem(y + dy, outer) * 2 + pc
        return remote(
            pbuf.at[p, group], prc.at[dy, p], pc_send.at[dy, p], pc_recv.at[dy, p], s, core
        )

    def share_plane(dy, p):
        return remote(
            pcs.at[dy, p], pry.at[dy, p], py_send.at[dy, p], py_recv.at[dy, p],
            s, lax.rem(y + dy, outer) * 2 + c,
        )

    parts = pbuf.shape[0]
    part_width = width // parts
    for p in range(parts + 1):
        if p < parts:
            piece = jnp.dot(
                att[...],
                ow[:, p * part_width:(p + 1) * part_width],
                preferred_element_type=jnp.float32,
            )
            pbuf[p] = piece.astype(jnp.bfloat16).reshape(tp, rows, part_width)
            for dy in list(range(1, outer)) + [0]:
                begin(share_pair(dy, p))
        if p >= 1:
            for dy in range(1, outer):
                share_pair(dy, p - 1).wait_recv()
                there = lax.rem(y + dy, outer) * 2 + c
                pcs[dy, p - 1] = (
                    pbuf[p - 1, there].astype(jnp.float32)
                    + prc[dy, p - 1].astype(jnp.float32)
                ).astype(jnp.bfloat16)
                begin(share_plane(dy, p - 1))
    summed = jnp.zeros((rows, 1), jnp.float32)
    for p in range(parts):
        columns = slice(p * part_width, (p + 1) * part_width)
        share_pair(0, p).wait_recv()
        piece = pbuf[p, t].astype(jnp.float32) + prc[0, p].astype(jnp.float32)
        piece = piece + res[:, columns].astype(jnp.float32)
        for dy in range(1, outer):
            share_plane(dy, p).wait_recv()
            piece = piece + pry[dy, p].astype(jnp.float32)
        total[:, columns] = piece
        summed += jnp.sum(piece, axis=-1, keepdims=True)
    centered = total[...] - summed / width
    variance = jnp.mean(centered * centered, axis=-1, keepdims=True)
    normed[...] = (centered * lax.rsqrt(variance + 1e-05) * ngain[...]).astype(jnp.bfloat16)

    @pl.loop(0, width // tile)
    def _(n):
        columns = pl.ds(pl.multiple_of(n * tile, tile), tile)
        piece = lax.dot_general(
            placed[...],
            normed[:, columns],
            (((0,), (0,)), ((), ())),
            preferred_element_type=jnp.float32,
        )
        outg[:, :, columns] = piece.astype(jnp.bfloat16).reshape(sp, cap, tile)

    tok[0, t] = outg[s]
    def arrive(k):
        there = lax.rem(s + k, sp)
        return remote(outg.at[there], tok.at[k, t], a_send.at[k], a_recv.at[k], there, t)

    def plane(k, dy):
        return remote(
            tok.at[k, t], tok.at[k, t], y_send.at[k, dy], y_recv.at[k, dy],
            s, lax.rem(y + dy, outer) * 2 + c,
        )

    def pair(k, dy):
        mine = lax.rem(y + outer - dy, outer) * 2 + c
        return remote(
            tok.at[k, mine], tok.at[k, mine], c_send.at[k, dy], c_recv.at[k, dy], s, core
        )

    def back_pair(k, dy):
        group = lax.rem(y + dy, outer) * 2 + pc
        return remote(
            part.at[k, group], rc.at[k, dy], rc_send.at[k, dy], rc_recv.at[k, dy], s, core
        )

    def back_plane(k, dy):
        return remote(
            cs.at[k, dy], ry.at[k, dy], ry_send.at[k, dy], ry_recv.at[k, dy],
            s, lax.rem(y + dy, outer) * 2 + c,
        )

    def back(k):
        there = lax.rem(s + sp - k, sp)
        return remote(fin.at[k], ret.at[s], ra_send.at[k], ra_recv.at[k], there, t)

    def landed_tok(k, group, send, recv):
        remote(tok.at[k, group], tok.at[k, group], send, recv, s, core).wait_recv()

    for k in range(1, sp):
        begin(arrive(k))

    def spread(first):
        for k in range(first, first + span):
            if k:
                landed_tok(k, t, a_send.at[k], a_recv.at[k])
            for dy in range(1, outer):
                begin(plane(k, dy))
            begin(pair(k, 0))

    def collect(first):
        for k in range(first, first + span):
            for dy in range(1, outer):
                group = lax.rem(y + outer - dy, outer) * 2
                landed_tok(k, group + c, y_send.at[k, dy], y_recv.at[k, dy])
                begin(pair(k, dy))
        for k in range(first, first + span):
            for dy in range(outer):
                group = lax.rem(y + outer - dy, outer) * 2
                landed_tok(k, group + pc, c_send.at[k, dy], c_recv.at[k, dy])

    def compute(first):
        count = span * tp * cap
        token_rows = tok[first:first + span].reshape(count, width)
        gated = jnp.dot(token_rows, gate[...], preferred_element_type=jnp.float32)
        upward = jnp.dot(token_rows, up[...], preferred_element_type=jnp.float32)
        hidden = (gated / (1.0 + jnp.exp(-gated)) * upward).astype(jnp.bfloat16)

        @pl.loop(0, width // tile)
        def _(n):
            columns = pl.ds(pl.multiple_of(n * tile, tile), tile)
            piece = jnp.dot(hidden, down[:, columns], preferred_element_type=jnp.float32)
            part[first:first + span, :, :, columns] = piece.astype(jnp.bfloat16).reshape(
                span, tp, cap, tile
            )

        for dy in list(range(1, outer)) + [0]:
            for k in range(first, first + span):
                begin(back_pair(k, dy))

    def reduce_pair(first):
        for k in range(first, first + span):
            for dy in range(1, outer):
                back_pair(k, dy).wait_recv()
                there = lax.rem(y + dy, outer) * 2 + c
                cs[k, dy] = (
                    part[k, there].astype(jnp.float32) + rc[k, dy].astype(jnp.float32)
                ).astype(jnp.bfloat16)
                begin(back_plane(k, dy))

    def reduce_plane(first):
        for k in range(first, first + span):
            back_pair(k, 0).wait_recv()
            whole = part[k, t].astype(jnp.float32) + rc[k, 0].astype(jnp.float32)
            for dy in range(1, outer):
                back_plane(k, dy).wait_recv()
                whole = whole + ry[k, dy].astype(jnp.float32)
            fin[k] = whole.astype(jnp.bfloat16)
            if k:
                begin(back(k))
            else:
                ret[s] = fin[k]

    firsts = list(range(0, sp, span))
    steps = len(firsts)
    lead, lag = 2, 2
    for step in range(min(lead, steps)):
        spread(firsts[step])
    for step in range(steps):
        collect(firsts[step])
        if step == 0:
            for copy in fetches:
                copy.wait()
        compute(firsts[step])
        reduce_pair(firsts[step])
        if step + lead < steps:
            spread(firsts[step + lead])
        if step >= lag:
            reduce_plane(firsts[step - lag])
    for step in range(max(steps - lag, 0), steps):
        reduce_plane(firsts[step])
    for k in range(1, sp):
        there = lax.rem(s + k, sp)
        remote(ret.at[there], ret.at[there], ra_send.at[k], ra_recv.at[k], s, core).wait_recv()

    mix_high = mix[...].astype(jnp.bfloat16)
    mix_low = (mix[...] - mix_high.astype(jnp.float32)).astype(jnp.bfloat16)

    @pl.loop(0, width // tile)
    def _(n):
        columns = pl.ds(pl.multiple_of(n * tile, tile), tile)
        returned = ret[:, :, columns].reshape(sp * cap, tile)
        combined = jnp.dot(mix_high, returned, preferred_element_type=jnp.float32)
        combined += jnp.dot(mix_low, returned, preferred_element_type=jnp.float32)
        out[:, columns] = (normed[:, columns].astype(jnp.float32) + combined).astype(
            jnp.bfloat16
        )

    for copy in sends:
        copy.wait_send()


def layer(
    query_one, key_one, query_two, key_two, value, lambda_head, head_gain, out_weight,
    residual, norm_gain, route_expert, route_weight, gate, up, down,
):
    sp, tp = lax.axis_size("sp"), lax.axis_size("tp")
    local = query_one.shape[0]
    heads = lambda_head.shape[0]
    kv_heads = key_one.shape[1] // HEAD
    rows, width = residual.shape
    hidden = gate.shape[1]
    cap = slots(rows, route_expert.shape[1], sp)
    outer, lanes = tp // 2, sp // 2
    span, parts = 1, 4
    vmem = pl.BlockSpec(memory_space=pltpu.VMEM)
    hbm = pl.BlockSpec(memory_space=pl.ANY)
    smem = pl.BlockSpec(memory_space=pltpu.SMEM)
    dma = pltpu.SemaphoreType.DMA
    bf16 = jnp.bfloat16
    return pl.pallas_call(
        functools.partial(layer_kernel, sp, tp, heads, kv_heads, cap, span),
        out_shape=jax.ShapeDtypeStruct((rows, width), bf16),
        in_specs=[vmem] * 5 + [smem, vmem, hbm] + [vmem] * 4 + [hbm] * 3,
        out_specs=vmem,
        scratch_shapes=[
            pltpu.VMEM((sp, local, 4 * kv_heads * HEAD), bf16),
            pltpu.VMEM(out_weight.shape, bf16),
            pltpu.VMEM((local, heads * 2 * HEAD), bf16),
            pltpu.VMEM((parts, tp, rows, width // parts), bf16),
            pltpu.VMEM((outer, parts, rows, width // parts), bf16),
            pltpu.VMEM((outer, parts, rows, width // parts), bf16),
            pltpu.VMEM((outer, parts, rows, width // parts), bf16),
            pltpu.VMEM((rows, width), jnp.float32),
            pltpu.VMEM((rows, width), bf16),
            pltpu.VMEM((rows, sp * cap), bf16),
            pltpu.VMEM((rows, sp * cap), jnp.float32),
            pltpu.VMEM((width, hidden), bf16),
            pltpu.VMEM((width, hidden), bf16),
            pltpu.VMEM((hidden, width), bf16),
            pltpu.VMEM((sp, cap, width), bf16),
            pltpu.VMEM((sp, tp, cap, width), bf16),
            pltpu.VMEM((sp, tp, cap, width), bf16),
            pltpu.VMEM((sp, outer, cap, width), bf16),
            pltpu.VMEM((sp, outer, cap, width), bf16),
            pltpu.VMEM((sp, outer, cap, width), bf16),
            pltpu.VMEM((sp, cap, width), bf16),
            pltpu.VMEM((sp, cap, width), bf16),
            dma, dma((lanes,)), dma((lanes,)), dma((lanes,)), dma((lanes,)),
            dma((outer, parts)), dma((outer, parts)), dma((outer, parts)), dma((outer, parts)),
            dma((3,)), dma((sp,)), dma((sp,)),
            dma((sp, outer)), dma((sp, outer)), dma((sp, outer)), dma((sp, outer)),
            dma((sp, outer)), dma((sp, outer)), dma((sp, outer)), dma((sp, outer)),
            dma((sp,)), dma((sp,)),
        ],
        compiler_params=pltpu.CompilerParams(
            collective_id=0, has_side_effects=True, vmem_limit_bytes=VMEM_BYTES
        ),
        name="layer",
    )(
        query_one, key_one, query_two, key_two, value, lambda_head,
        head_gain[None, :], out_weight, residual, norm_gain[None, :],
        route_expert, route_weight, gate, up, down,
    )


def on_device_kernels(*arrays):
    return layer(*arrays[:12], *(weight[0] for weight in arrays[12:]))


def slots(rows, top_count, experts):
    return max(2 * rows * top_count // experts, 2)


def fits(*arrays):
    query_one, residual, route_expert = arrays[0], arrays[8], arrays[10]
    sp, tp = lax.axis_size("sp"), lax.axis_size("tp")
    rows, top_count = route_expert.shape
    return (
        sp % 2 == 0
        and tp % 2 == 0
        and slots(rows, top_count, sp) % 16 == 0
        and rows % 16 == 0
        and query_one.shape[0] * sp <= 2048
        and residual.shape[1] % 512 == 0
        and sp <= 8
    )


def on_device(*arrays):
    if fits(*arrays):
        return on_device_kernels(*arrays)
    return on_device_collectives(*arrays)


def on_device_collectives(
    query_one,
    key_one,
    query_two,
    key_two,
    value,
    lambda_head,
    head_gain,
    out_weight,
    residual,
    norm_gain,
    route_expert,
    route_weight,
    expert_gate,
    expert_up,
    expert_down,
):
    local_tokens = query_one.shape[0]
    heads_here = lambda_head.shape[0]
    kv_here = key_one.shape[1] // HEAD
    per_key = heads_here // kv_here
    offset = lax.axis_index("sp") * local_tokens
    first_queries = query_one.reshape(local_tokens, kv_here, per_key, HEAD)
    second_queries = query_two.reshape(local_tokens, kv_here, per_key, HEAD)
    query_pos = offset + jnp.arange(local_tokens, dtype=jnp.int32)

    def initial():
        return (
            jnp.full((kv_here, per_key, local_tokens), -1e30, jnp.float32),
            jnp.zeros((kv_here, per_key, local_tokens), jnp.float32),
            jnp.zeros((local_tokens, kv_here, per_key, 2 * HEAD), jnp.float32),
        )

    carried = (initial(), initial())
    key_first = lax.all_gather(key_one, "sp", axis=0, tiled=True)
    key_second = lax.all_gather(key_two, "sp", axis=0, tiled=True)
    value_rows = lax.all_gather(value, "sp", axis=0, tiled=True)
    length = key_first.shape[0]
    key_width = math.gcd(length, 1024)

    def advance(block_index, carried):
        block_start = block_index * key_width

        def attend(carried):
            first_block = lax.dynamic_slice_in_dim(key_first, block_start, key_width, 0)
            second_block = lax.dynamic_slice_in_dim(key_second, block_start, key_width, 0)
            value_block = lax.dynamic_slice_in_dim(value_rows, block_start, key_width, 0)
            first_block = first_block.reshape(key_width, kv_here, HEAD)
            second_block = second_block.reshape(key_width, kv_here, HEAD)
            value_block = value_block.reshape(key_width, kv_here, 2 * HEAD)
            key_pos = block_start + jnp.arange(key_width, dtype=jnp.int32)
            allowed = key_pos[None, :] <= query_pos[:, None]
            return (
                map_step(carried[0], first_queries, first_block, value_block, allowed),
                map_step(carried[1], second_queries, second_block, value_block, allowed),
            )

        def unchanged(carried):
            return carried

        return lax.cond(block_start <= offset + local_tokens - 1, attend, unchanged, carried)

    state_one, state_two = lax.fori_loop(0, length // key_width, advance, carried)
    difference = finish(state_one) - lambda_head.reshape(kv_here, per_key)[
        None, :, :, None
    ] * finish(state_two)
    scaled = (
        difference
        * lax.rsqrt(jnp.mean(difference * difference, axis=-1, keepdims=True) + 1e-05)
        * head_gain
    )
    attended = scaled.astype(jnp.bfloat16).reshape(local_tokens, heads_here * 2 * HEAD)
    own_rows = residual.shape[0]
    projected = lax.psum_scatter(
        jnp.dot(attended, out_weight, preferred_element_type=jnp.float32).astype(jnp.bfloat16),
        "tp",
        scatter_dimension=0,
        tiled=True,
    ).astype(jnp.float32)
    summed_in = residual.astype(jnp.float32) + projected
    centered = summed_in - jnp.mean(summed_in, axis=-1, keepdims=True)
    variance = jnp.mean(centered * centered, axis=-1, keepdims=True)
    normed = (centered * lax.rsqrt(variance + 1e-05) * norm_gain).astype(jnp.bfloat16)
    experts = lax.axis_size("sp")
    tp_count = lax.axis_size("tp")
    model_width = normed.shape[1]
    top_count = route_expert.shape[1]
    capacity = max(2 * own_rows * top_count // experts, 2)
    chosen = route_expert.reshape(own_rows * top_count)
    onehot = (chosen[:, None] == jnp.arange(experts, dtype=jnp.int32)[None, :]).astype(jnp.int32)
    slot_index = jnp.sum((jnp.cumsum(onehot, axis=0) - onehot) * onehot, axis=1)
    target = chosen * capacity + slot_index
    placed = target[:, None] == jnp.arange(experts * capacity, dtype=jnp.int32)[None, :]
    placed = jnp.any(placed.reshape(own_rows, top_count, experts * capacity), axis=1).astype(
        jnp.bfloat16
    )
    outgoing = jnp.einsum("rp,rd->pd", placed, normed, preferred_element_type=jnp.float32)
    outgoing = outgoing.astype(jnp.bfloat16).reshape(experts, capacity, model_width)
    arrived = lax.all_to_all(outgoing, "sp", split_axis=0, concat_axis=0, tiled=True)
    all_rows = lax.all_gather(arrived, "tp", axis=0, tiled=True)
    token_rows = all_rows.reshape(-1, model_width)
    gated = jnp.dot(token_rows, expert_gate[0], preferred_element_type=jnp.float32)
    upward = jnp.dot(token_rows, expert_up[0], preferred_element_type=jnp.float32)
    hidden = (jax.nn.silu(gated) * upward).astype(jnp.bfloat16)
    partial_value = (
        jnp.dot(hidden, expert_down[0], preferred_element_type=jnp.float32)
        .astype(jnp.bfloat16)
        .reshape(tp_count, experts * capacity, model_width)
    )
    summed = (
        lax.psum_scatter(partial_value, "tp", scatter_dimension=0, tiled=True)
        .astype(jnp.float32)
        .reshape(experts, capacity, model_width)
    )
    returned = lax.all_to_all(
        summed.astype(jnp.bfloat16), "sp", split_axis=0, concat_axis=0, tiled=True
    )
    picked = returned.reshape(experts * capacity, model_width)[target]
    picked = picked.reshape(own_rows, top_count, model_width).astype(jnp.float32)
    combined = jnp.sum(route_weight[:, :, None] * picked, axis=1)
    return (normed.astype(jnp.float32) + combined).astype(jnp.bfloat16)


def solution(mesh):
    in_specs = (
        P("sp", "tp"),
        P("sp", "tp"),
        P("sp", "tp"),
        P("sp", "tp"),
        P("sp", "tp"),
        P("tp"),
        P(),
        P("tp", None),
        P(("sp", "tp"), None),
        P(),
        P(("sp", "tp"), None),
        P(("sp", "tp"), None),
        P("sp", None, "tp"),
        P("sp", None, "tp"),
        P("sp", "tp", None),
    )
    out_specs = P(("sp", "tp"), None)
    return jax.shard_map(
        on_device, mesh=mesh, in_specs=in_specs, out_specs=out_specs, check_vma=False
    )
```

profile of v0, /device:TPU:0, one launch (start us, length us, event | category | flops | bytes accessed | tf_op | source)
XLA Modules:
  0.0 110.8 jit_solution(8528117361297743920)
XLA Ops:
  0.0 1.4 %copy.16.route_e = s32[32,2]{1,0:T(8,128)} copy(s32[32,2]{0,1:T(2,128)} %param.25) | data formatting | bytes 512 | tf_op args[10]
  1.4 1.4 %copy.17.route_w = f32[32,2]{1,0:T(8,128)} copy(f32[32,2]{0,1:T(2,128)} %param.26) | data formatting | bytes 512 | tf_op args[11]
  2.7 106.4 %layer.1 = bf16[32,4096]{1,0:T(8,128)(2,1)} custom-call(bf16[128,256]{1,0:T(8,128)(2,1)} %q1.1, bf16[128,128]{1,0:T(8,128)(2,1)} %k1.1, bf16[128,256]{1,0:T(8,128)(2,1)} %q2.1, bf16[128,128]{1,0:T(8,128)(2,1)} %k2.1, bf16[128,256]{1,0:T(8,128)(2,1)} %v.1, f32[2]{0:T(128)} %lam.1, f32[1,256]{1,0:T(1,128)} %bitcast.9, bf16[512,4096]{1,0:T(8,128)(2,1)} %ow_hbm.1, ...), custom_call_target="tpu_custom_call" | custom-call | tf_op jit(solution)/shard_map/layer/pallas_call | solution.py:404
  109.1 1.7 %copy.19 = bf16[32,4096]{1,0:T(8,128)(2,1)} copy(bf16[32,4096]{1,0:T(8,128)(2,1)} %layer.1) | data formatting | bytes 524288
where the time goes:
time: 111 us
  Pallas kernels  106 us (95%)
  local copies, waits for them, and re-layouts  4.39 us (4%)
    pallas_call x1, Pallas kernels, layer(): pl.pallas_call(functools.partial(layer_kernel, sp, tp, heads, kv_heads, c...  106 us
    unnamed x3, local copies, waits for them, and re-layouts  4.39 us

commit v1 on v0

--- a/solution.py
+++ b/solution.py
@@ -10,6 +10,7 @@
 
 HEAD = 128
 VMEM_BYTES = 58 * 1024 * 1024
+CHUNKS, EARLY = 4, 3
 
 
 def map_step(carried, query_rows, key_block, value_block, allowed):
@@ -47,8 +48,44 @@
     )
 
 
-def greet(peers):
+def flipped(index, mask):
+    bit = 1
+    while bit <= mask:
+        if mask & bit:
+            index = index + bit - 2 * bit * lax.rem(lax.div(index, bit), 2)
+        bit *= 2
+    return index
+
+
+def layer_kernel(
+    sp, tp, heads, kv_heads, cap, early,
+    q1_hbm, k1_hbm, q2_hbm, k2_hbm, v_hbm, lam, gain, ow_hbm, res_hbm, ngain,
+    route_e, route_w, gate_hbm, up_hbm, down_hbm, out,
+    q1, q2, res, kv, ow, att, pbuf, prc, pcs, pry, total, normed, placed, mix,
+    gate, up, down, moved, hid, hidr, outg, tok, part, rc, cs, ry, fin, ret,
+    f_sem, z_send, z_recv, x_send, x_recv, pc_send, pc_recv, py_send, py_recv,
+    d_send, d_recv, h_send, h_recv, a_send, a_recv, y_send, y_recv, c_send, c_recv,
+    rc_send, rc_recv, ry_send, ry_recv, ra_send, ra_recv,
+):
+    s = lax.axis_index("sp")
+    t = lax.axis_index("tp")
+    z, x = lax.div(s, 2), lax.rem(s, 2)
+    y, c = lax.div(t, 2), lax.rem(t, 2)
+    lanes = sp // 2
+    px = flipped(s, 1)
+    core = flipped(t, 1)
+    plane_peer = flipped(t, 2)
+    corner = flipped(t, 3)
+    local = q1.shape[0]
+    rows, width = out.shape
+    kw = kv_heads * HEAD
+    chunks, chunk = moved.shape[0], moved.shape[3]
+    shared = chunks * chunk
+    own_part = width - shared
+
     barrier = pltpu.get_barrier_semaphore()
+    peers = [(flipped(s, k), t) for k in range(1, sp)]
+    peers += [(s, flipped(t, r)) for r in range(1, tp)]
     for sp_to, tp_to in peers:
         pl.semaphore_signal(
             barrier,
@@ -56,95 +93,102 @@
             device_id={"sp": sp_to, "tp": tp_to},
             device_id_type=pl.DeviceIdType.MESH,
         )
-    pl.semaphore_wait(barrier, len(peers))
-
-
-def tp_place(tp):
-    t = lax.axis_index("tp")
-    c = lax.rem(t, 2)
-    y = lax.div(t, 2)
-    return t, y, c, 1 - c
-
-
-def layer_kernel(
-    sp, tp, heads, kv_heads, cap, span,
-    q1, k1, q2, k2, v, lam, gain, ow_hbm, res, ngain, route_e, route_w,
-    gate_hbm, up_hbm, down_hbm, out,
-    kv, ow, att, pbuf, prc, pcs, pry, total, normed, placed, mix,
-    gate, up, down, outg, tok, part, rc, cs, ry, fin, ret,
-    ow_sem, z_send, z_recv, x_send, x_recv, pc_send, pc_recv, py_send, py_recv,
-    w_sem, a_send, a_recv, y_send, y_recv, c_send, c_recv,
-    rc_send, rc_recv, ry_send, ry_recv, ra_send, ra_recv,
-):
-    s = lax.axis_index("sp")
-    t, y, c, pc = tp_place(tp)
-    outer = tp // 2
-    lanes = sp // 2
-    px = s + 1 - 2 * lax.rem(s, 2)
-    local = q1.shape[0]
-    rows, width = out.shape
-    tile = math.gcd(width, 512)
-    core = y * 2 + pc
-    kw = kv_heads * HEAD
-    fetch = pltpu.make_async_copy(ow_hbm, ow, ow_sem)
-    fetch.start()
+    sources = [
+        (k1_hbm, kv.at[s, :, 0:kw]), (k2_hbm, kv.at[s, :, kw:2 * kw]),
+        (v_hbm, kv.at[s, :, 2 * kw:4 * kw]), (down_hbm, down), (q1_hbm, q1), (q2_hbm, q2),
+        (ow_hbm, ow), (res_hbm, res), (gate_hbm, gate), (up_hbm, up),
+    ]
     fetches = [
-        pltpu.make_async_copy(gate_hbm, gate, w_sem.at[0]),
-        pltpu.make_async_copy(up_hbm, up, w_sem.at[1]),
-        pltpu.make_async_copy(down_hbm, down, w_sem.at[2]),
+        pltpu.make_async_copy(src, dst, f_sem.at[i]) for i, (src, dst) in enumerate(sources)
     ]
     for copy in fetches:
         copy.start()
-    kv[s, :, 0:kw] = k1[...]
-    kv[s, :, kw:2 * kw] = k2[...]
-    kv[s, :, 2 * kw:4 * kw] = v[...]
-    peers = [(lax.rem(s + k, sp), t) for k in range(1, sp)] + [(s, core)]
-    peers += [(s, lax.rem(y + dy, outer) * 2 + c) for dy in range(1, outer)]
-    greet(peers)
-    sends = []
-    for m in range(1, lanes):
-        copy = remote(
-            kv.at[s], kv.at[s], z_send.at[m], z_recv.at[m], lax.rem(s + 2 * m, sp), t
-        )
-        copy.start()
-        sends.append(copy)
-
-    def across(m):
-        block = lax.rem(s + sp - 2 * m, sp)
-        return remote(kv.at[block], kv.at[block], x_send.at[m], x_recv.at[m], px, t)
-
-    places = lax.broadcasted_iota(jnp.int32, (rows, sp * cap), 1).astype(jnp.float32)
+    for block in range(1, sp):
+        @pl.when(block > s)
+        def _():
+            kv[block] = jnp.zeros(kv.shape[1:], kv.dtype)
+
+    places = lax.broadcasted_iota(jnp.int32, (sp * cap, rows), 0).astype(jnp.float32)
     owner = jnp.floor((places + 0.5) / cap)
     slot = places - owner * cap
-    named = jnp.zeros((rows, sp * cap), jnp.float32)
-    share = jnp.zeros((rows, sp * cap), jnp.float32)
-    for choice in range(route_e.shape[1]):
-        match = route_e[:, choice:choice + 1].astype(jnp.float32) == owner
+    named = jnp.zeros((sp * cap, rows), jnp.float32)
+    share = jnp.zeros((sp * cap, rows), jnp.float32)
+    for choice in range(route_e.shape[0]):
+        match = route_e[choice:choice + 1, :].astype(jnp.float32) == owner
         named += jnp.where(match, 1.0, 0.0)
-        share += jnp.where(match, route_w[:, choice:choice + 1], 0.0)
-    earlier = lax.broadcasted_iota(jnp.int32, (rows, rows), 1) < lax.broadcasted_iota(
-        jnp.int32, (rows, rows), 0
+        share += jnp.where(match, route_w[choice:choice + 1, :], 0.0)
+    earlier = lax.broadcasted_iota(jnp.int32, (rows, rows), 0) < lax.broadcasted_iota(
+        jnp.int32, (rows, rows), 1
     )
     rank = jnp.dot(
+        named.astype(jnp.bfloat16),
         jnp.where(earlier, 1.0, 0.0).astype(jnp.bfloat16),
-        named.astype(jnp.bfloat16),
         preferred_element_type=jnp.float32,
     )
     held = jnp.where(rank == slot, named, 0.0)
     placed[...] = held.astype(jnp.bfloat16)
     mix[...] = share * held
 
-    for m in range(lanes):
-        if m:
-            block = lax.rem(s + sp - 2 * m, sp)
-            remote(kv.at[block], kv.at[block], z_send.at[m], z_recv.at[m], px, t).wait_recv()
-        copy = across(m)
+    sends = []
+
+    def begin(copy):
         copy.start()
         sends.append(copy)
-    for m in range(lanes):
-        block = lax.rem(px + sp - 2 * m, sp)
-        remote(kv.at[block], kv.at[block], x_send.at[m], x_recv.at[m], px, t).wait_recv()
-
+
+    def along(block, to, d):
+        return remote(kv.at[block], kv.at[block], z_send.at[d], z_recv.at[d], to, t)
+
+    def across(block, d):
+        return remote(kv.at[block], kv.at[block], x_send.at[d], x_recv.at[d], px, t)
+
+    for copy in fetches[:3]:
+        copy.wait()
+    pl.semaphore_wait(barrier, len(peers))
+    for d in (2, 1):
+        @pl.when(z + d < lanes)
+        def _():
+            along(s, s + 2 * d, d).start()
+
+    @pl.when(x == 0)
+    def _():
+        across(s, 0).start()
+
+    def lend(n, r):
+        to = flipped(t, r)
+        columns = slice(n * chunk, (n + 1) * chunk)
+        return remote(
+            down.at[:, columns], moved.at[n, r - 1], d_send.at[n, r - 1], d_recv.at[n, r - 1],
+            s, to,
+        )
+
+    def relend(n):
+        return remote(
+            moved.at[n, 1], moved.at[n, 2], d_send.at[n, 2], d_recv.at[n, 2], s, core
+        )
+
+    fetches[3].wait()
+    for n in range(early):
+        begin(lend(n, 2))
+    for n in range(chunks):
+        begin(lend(n, 1))
+
+    for level, order in ((1, (1,)), (2, (2, 1)), (3, (1, 2, 3))):
+        @pl.when(z == level)
+        def _():
+            for d in order:
+                along(s - 2 * d, s, d).wait_recv()
+                if level + d == 4 and d == 2:
+                    along(s - 2 * d, s + 2, 3).start()
+                across(s - 2 * d, d).start()
+            for d in order:
+                across(px - 2 * d, d).wait_recv()
+
+    @pl.when(x == 1)
+    def _():
+        across(px, 0).wait_recv()
+
+    for copy in fetches[4:6]:
+        copy.wait()
     length = sp * local
     key_pos = lax.broadcasted_iota(jnp.int32, (local, length), 1)
     query_pos = s * local + lax.broadcasted_iota(jnp.int32, (local, length), 0)
@@ -179,23 +223,16 @@
         )
         att[:, h * 2 * HEAD:(h + 1) * 2 * HEAD] = scaled.astype(jnp.bfloat16)
 
-    fetch.wait()
-
-    def begin(copy):
-        copy.start()
-        sends.append(copy)
-
-    def share_pair(dy, p):
-        group = lax.rem(y + dy, outer) * 2 + pc
+    fetches[6].wait()
+
+    def share_pair(there, dy, p):
+        group = flipped(core, 2) if dy else core
         return remote(
             pbuf.at[p, group], prc.at[dy, p], pc_send.at[dy, p], pc_recv.at[dy, p], s, core
         )
 
-    def share_plane(dy, p):
-        return remote(
-            pcs.at[dy, p], pry.at[dy, p], py_send.at[dy, p], py_recv.at[dy, p],
-            s, lax.rem(y + dy, outer) * 2 + c,
-        )
+    def share_plane(p):
+        return remote(pcs.at[p], pry.at[p], py_send.at[p], py_recv.at[p], s, plane_peer)
 
     parts = pbuf.shape[0]
     part_width = width // parts
@@ -207,167 +244,188 @@
                 preferred_element_type=jnp.float32,
             )
             pbuf[p] = piece.astype(jnp.bfloat16).reshape(tp, rows, part_width)
-            for dy in list(range(1, outer)) + [0]:
-                begin(share_pair(dy, p))
+            for dy in (1, 0):
+                begin(share_pair(None, dy, p))
         if p >= 1:
-            for dy in range(1, outer):
-                share_pair(dy, p - 1).wait_recv()
-                there = lax.rem(y + dy, outer) * 2 + c
-                pcs[dy, p - 1] = (
-                    pbuf[p - 1, there].astype(jnp.float32)
-                    + prc[dy, p - 1].astype(jnp.float32)
-                ).astype(jnp.bfloat16)
-                begin(share_plane(dy, p - 1))
+            share_pair(None, 1, p - 1).wait_recv()
+            pcs[p - 1] = (
+                pbuf[p - 1, plane_peer].astype(jnp.float32) + prc[1, p - 1].astype(jnp.float32)
+            ).astype(jnp.bfloat16)
+            begin(share_plane(p - 1))
+    for n in range(early, chunks):
+        begin(lend(n, 2))
+    fetches[7].wait()
     summed = jnp.zeros((rows, 1), jnp.float32)
     for p in range(parts):
         columns = slice(p * part_width, (p + 1) * part_width)
-        share_pair(0, p).wait_recv()
+        share_pair(None, 0, p).wait_recv()
         piece = pbuf[p, t].astype(jnp.float32) + prc[0, p].astype(jnp.float32)
         piece = piece + res[:, columns].astype(jnp.float32)
-        for dy in range(1, outer):
-            share_plane(dy, p).wait_recv()
-            piece = piece + pry[dy, p].astype(jnp.float32)
+        share_plane(p).wait_recv()
+        piece = piece + pry[p].astype(jnp.float32)
         total[:, columns] = piece
         summed += jnp.sum(piece, axis=-1, keepdims=True)
     centered = total[...] - summed / width
     variance = jnp.mean(centered * centered, axis=-1, keepdims=True)
     normed[...] = (centered * lax.rsqrt(variance + 1e-05) * ngain[...]).astype(jnp.bfloat16)
 
+    tile = math.gcd(width, 1024)
+
     @pl.loop(0, width // tile)
     def _(n):
         columns = pl.ds(pl.multiple_of(n * tile, tile), tile)
-        piece = lax.dot_general(
-            placed[...],
-            normed[:, columns],
-            (((0,), (0,)), ((), ())),
-            preferred_element_type=jnp.float32,
-        )
+        piece = jnp.dot(placed[...], normed[:, columns], preferred_element_type=jnp.float32)
         outg[:, :, columns] = piece.astype(jnp.bfloat16).reshape(sp, cap, tile)
 
-    tok[0, t] = outg[s]
     def arrive(k):
-        there = lax.rem(s + k, sp)
+        there = flipped(s, k)
         return remote(outg.at[there], tok.at[k, t], a_send.at[k], a_recv.at[k], there, t)
 
-    def plane(k, dy):
+    def plane(k):
         return remote(
-            tok.at[k, t], tok.at[k, t], y_send.at[k, dy], y_recv.at[k, dy],
-            s, lax.rem(y + dy, outer) * 2 + c,
+            tok.at[k, t], tok.at[k, t], y_send.at[k], y_recv.at[k], s, plane_peer
         )
 
     def pair(k, dy):
-        mine = lax.rem(y + outer - dy, outer) * 2 + c
+        mine = plane_peer if dy else t
         return remote(
             tok.at[k, mine], tok.at[k, mine], c_send.at[k, dy], c_recv.at[k, dy], s, core
         )
 
     def back_pair(k, dy):
-        group = lax.rem(y + dy, outer) * 2 + pc
+        group = corner if dy else core
         return remote(
             part.at[k, group], rc.at[k, dy], rc_send.at[k, dy], rc_recv.at[k, dy], s, core
         )
 
-    def back_plane(k, dy):
+    def back_plane(k):
+        return remote(cs.at[k], ry.at[k], ry_send.at[k], ry_recv.at[k], s, plane_peer)
+
+    def pass_hidden(k, r):
+        to = flipped(t, r)
         return remote(
-            cs.at[k, dy], ry.at[k, dy], ry_send.at[k, dy], ry_recv.at[k, dy],
-            s, lax.rem(y + dy, outer) * 2 + c,
+            hid.at[k, to], hidr.at[k, r], h_send.at[k, r - 1], h_recv.at[k, r - 1], s, to
         )
 
     def back(k):
-        there = lax.rem(s + sp - k, sp)
-        return remote(fin.at[k], ret.at[s], ra_send.at[k], ra_recv.at[k], there, t)
+        return remote(fin.at[k], ret.at[s], ra_send.at[k], ra_recv.at[k], flipped(s, k), t)
 
     def landed_tok(k, group, send, recv):
         remote(tok.at[k, group], tok.at[k, group], send, recv, s, core).wait_recv()
 
-    for k in range(1, sp):
-        begin(arrive(k))
-
-    def spread(first):
-        for k in range(first, first + span):
-            if k:
-                landed_tok(k, t, a_send.at[k], a_recv.at[k])
-            for dy in range(1, outer):
-                begin(plane(k, dy))
-            begin(pair(k, 0))
-
-    def collect(first):
-        for k in range(first, first + span):
-            for dy in range(1, outer):
-                group = lax.rem(y + outer - dy, outer) * 2
-                landed_tok(k, group + c, y_send.at[k, dy], y_recv.at[k, dy])
-                begin(pair(k, dy))
-        for k in range(first, first + span):
-            for dy in range(outer):
-                group = lax.rem(y + outer - dy, outer) * 2
-                landed_tok(k, group + pc, c_send.at[k, dy], c_recv.at[k, dy])
-
-    def compute(first):
-        count = span * tp * cap
-        token_rows = tok[first:first + span].reshape(count, width)
+    order = step_order(sp)
+    for k in order:
+        if k:
+            begin(arrive(k))
+    tok[0, t] = outg[s]
+
+    def spread(k):
+        if k:
+            landed_tok(k, t, a_send.at[k], a_recv.at[k])
+        begin(plane(k))
+        begin(pair(k, 0))
+
+    def collect(k):
+        landed_tok(k, plane_peer, y_send.at[k], y_recv.at[k])
+        begin(pair(k, 1))
+        landed_tok(k, core, c_send.at[k, 0], c_recv.at[k, 0])
+        landed_tok(k, corner, c_send.at[k, 1], c_recv.at[k, 1])
+
+    def compute(k):
+        token_rows = tok[k].reshape(tp * cap, width)
         gated = jnp.dot(token_rows, gate[...], preferred_element_type=jnp.float32)
         upward = jnp.dot(token_rows, up[...], preferred_element_type=jnp.float32)
         hidden = (gated / (1.0 + jnp.exp(-gated)) * upward).astype(jnp.bfloat16)
-
-        @pl.loop(0, width // tile)
+        hid[k] = hidden.reshape(tp, cap, hidden.shape[1])
+        hidr[k, 0] = hid[k, t]
+        for r in range(1, tp):
+            begin(pass_hidden(k, r))
+        step = math.gcd(own_part, 512)
+
+        @pl.loop(0, own_part // step)
         def _(n):
-            columns = pl.ds(pl.multiple_of(n * tile, tile), tile)
-            piece = jnp.dot(hidden, down[:, columns], preferred_element_type=jnp.float32)
-            part[first:first + span, :, :, columns] = piece.astype(jnp.bfloat16).reshape(
-                span, tp, cap, tile
+            start = pl.multiple_of(n * step, step)
+            piece = jnp.dot(
+                hidden,
+                down[:, pl.ds(pl.multiple_of(shared + start, step), step)],
+                preferred_element_type=jnp.float32,
             )
-
-        for dy in list(range(1, outer)) + [0]:
-            for k in range(first, first + span):
-                begin(back_pair(k, dy))
-
-    def reduce_pair(first):
-        for k in range(first, first + span):
-            for dy in range(1, outer):
-                back_pair(k, dy).wait_recv()
-                there = lax.rem(y + dy, outer) * 2 + c
-                cs[k, dy] = (
-                    part[k, there].astype(jnp.float32) + rc[k, dy].astype(jnp.float32)
-                ).astype(jnp.bfloat16)
-                begin(back_plane(k, dy))
-
-    def reduce_plane(first):
-        for k in range(first, first + span):
+            part[k, :, :, pl.ds(start, step)] = piece.astype(jnp.bfloat16).reshape(tp, cap, step)
+
+        for dy in (1, 0):
+            begin(back_pair(k, dy))
+
+    def reduce_pair(k):
+        back_pair(k, 1).wait_recv()
+        cs[k] = (
+            part[k, plane_peer].astype(jnp.float32) + rc[k, 1].astype(jnp.float32)
+        ).astype(jnp.bfloat16)
+        begin(back_plane(k))
+
+    def finish_steps(ks):
+        for k in ks:
+            for r in range(1, tp):
+                pass_hidden(k, r).wait_recv()
+        lefts = [jnp.concatenate([hidr[k, r] for k in ks], axis=0) for r in range(tp)]
+        for n in range(chunks):
+            columns = slice(n * chunk, (n + 1) * chunk)
+            piece = jnp.dot(lefts[0], down[:, columns], preferred_element_type=jnp.float32)
+            for r in range(1, tp):
+                piece += jnp.dot(lefts[r], moved[n, r - 1], preferred_element_type=jnp.float32)
+            piece = piece.astype(jnp.bfloat16)
+            for i, k in enumerate(ks):
+                fin[k, :, columns] = piece[i * cap:(i + 1) * cap]
+        for k in ks:
             back_pair(k, 0).wait_recv()
             whole = part[k, t].astype(jnp.float32) + rc[k, 0].astype(jnp.float32)
-            for dy in range(1, outer):
-                back_plane(k, dy).wait_recv()
-                whole = whole + ry[k, dy].astype(jnp.float32)
-            fin[k] = whole.astype(jnp.bfloat16)
+            back_plane(k).wait_recv()
+            whole = whole + ry[k].astype(jnp.float32)
+            fin[k, :, shared:] = whole.astype(jnp.bfloat16)
             if k:
                 begin(back(k))
             else:
                 ret[s] = fin[k]
 
-    firsts = list(range(0, sp, span))
-    steps = len(firsts)
-    lead, lag = 2, 2
-    for step in range(min(lead, steps)):
-        spread(firsts[step])
-    for step in range(steps):
-        collect(firsts[step])
-        if step == 0:
-            for copy in fetches:
+    lead = 2
+    for k in order[:lead]:
+        spread(k)
+    for i, k in enumerate(order):
+        if i == 0:
+            for n in range(chunks):
+                lend(n, 2).wait_recv()
+                begin(relend(n))
+        collect(k)
+        if i == 0:
+            for copy in fetches[8:10]:
                 copy.wait()
-        compute(firsts[step])
-        reduce_pair(firsts[step])
-        if step + lead < steps:
-            spread(firsts[step + lead])
-        if step >= lag:
-            reduce_plane(firsts[step - lag])
-    for step in range(max(steps - lag, 0), steps):
-        reduce_plane(firsts[step])
+        compute(k)
+        if i == 1:
+            for n in range(chunks):
+                lend(n, 1).wait_recv()
+                relend(n).wait_recv()
+        if i % 2 and i > 1:
+            finish_steps(order[i - 3:i - 1])
+        reduce_pair(k)
+        if i + lead < len(order):
+            spread(order[i + lead])
+    finish_steps(order[-2:])
     for k in range(1, sp):
-        there = lax.rem(s + k, sp)
+        there = flipped(s, k)
         remote(ret.at[there], ret.at[there], ra_send.at[k], ra_recv.at[k], s, core).wait_recv()
 
-    mix_high = mix[...].astype(jnp.bfloat16)
-    mix_low = (mix[...] - mix_high.astype(jnp.float32)).astype(jnp.bfloat16)
+    unit = lax.broadcasted_iota(jnp.int32, (sp * cap, sp * cap), 0) == lax.broadcasted_iota(
+        jnp.int32, (sp * cap, sp * cap), 1
+    )
+    unit = jnp.where(unit, 1.0, 0.0).astype(jnp.bfloat16)
+
+    def turned(table):
+        return lax.dot_general(
+            table, unit, (((0,), (0,)), ((), ())), preferred_element_type=jnp.float32
+        ).astype(jnp.bfloat16)
+
+    high = mix[...].astype(jnp.bfloat16)
+    mix_low = turned((mix[...] - high.astype(jnp.float32)).astype(jnp.bfloat16))
+    mix_high = turned(high)
 
     @pl.loop(0, width // tile)
     def _(n):
@@ -381,6 +439,27 @@
 
     for copy in sends:
         copy.wait_send()
+    for d in (2, 1):
+        @pl.when(z + d < lanes)
+        def _():
+            along(s, s + 2 * d, d).wait_send()
+
+    @pl.when(x == 0)
+    def _():
+        across(s, 0).wait_send()
+
+    for level, order_of in ((1, (1,)), (2, (2, 1)), (3, (1, 2, 3))):
+        @pl.when(z == level)
+        def _():
+            for d in order_of:
+                if level + d == 4 and d == 2:
+                    along(s - 2 * d, s + 2, 3).wait_send()
+                across(s - 2 * d, d).wait_send()
+
+
+def step_order(sp):
+    far = [k for half in (3, 2) for k in (2 * half, 2 * half + 1)]
+    return [0, 1, 2] + far + [3]
 
 
 def layer(
@@ -394,47 +473,54 @@
     rows, width = residual.shape
     hidden = gate.shape[1]
     cap = slots(rows, route_expert.shape[1], sp)
-    outer, lanes = tp // 2, sp // 2
-    span, parts = 1, 4
+    lanes, parts = sp // 2, 4
+    chunk = width // 8
+    chunks, early = CHUNKS, EARLY
+    own_part = width - chunks * chunk
     vmem = pl.BlockSpec(memory_space=pltpu.VMEM)
     hbm = pl.BlockSpec(memory_space=pl.ANY)
     smem = pl.BlockSpec(memory_space=pltpu.SMEM)
     dma = pltpu.SemaphoreType.DMA
     bf16 = jnp.bfloat16
     return pl.pallas_call(
-        functools.partial(layer_kernel, sp, tp, heads, kv_heads, cap, span),
+        functools.partial(layer_kernel, sp, tp, heads, kv_heads, cap, early),
         out_shape=jax.ShapeDtypeStruct((rows, width), bf16),
-        in_specs=[vmem] * 5 + [smem, vmem, hbm] + [vmem] * 4 + [hbm] * 3,
+        in_specs=[hbm] * 5 + [smem, vmem, hbm, hbm] + [vmem] * 3 + [hbm] * 3,
         out_specs=vmem,
         scratch_shapes=[
+            pltpu.VMEM(query_one.shape, bf16),
+            pltpu.VMEM(query_two.shape, bf16),
+            pltpu.VMEM(residual.shape, bf16),
             pltpu.VMEM((sp, local, 4 * kv_heads * HEAD), bf16),
             pltpu.VMEM(out_weight.shape, bf16),
             pltpu.VMEM((local, heads * 2 * HEAD), bf16),
             pltpu.VMEM((parts, tp, rows, width // parts), bf16),
-            pltpu.VMEM((outer, parts, rows, width // parts), bf16),
-            pltpu.VMEM((outer, parts, rows, width // parts), bf16),
-            pltpu.VMEM((outer, parts, rows, width // parts), bf16),
+            pltpu.VMEM((2, parts, rows, width // parts), bf16),
+            pltpu.VMEM((parts, rows, width // parts), bf16),
+            pltpu.VMEM((parts, rows, width // parts), bf16),
             pltpu.VMEM((rows, width), jnp.float32),
             pltpu.VMEM((rows, width), bf16),
-            pltpu.VMEM((rows, sp * cap), bf16),
-            pltpu.VMEM((rows, sp * cap), jnp.float32),
+            pltpu.VMEM((sp * cap, rows), bf16),
+            pltpu.VMEM((sp * cap, rows), jnp.float32),
             pltpu.VMEM((width, hidden), bf16),
             pltpu.VMEM((width, hidden), bf16),
             pltpu.VMEM((hidden, width), bf16),
+            pltpu.VMEM((chunks, tp - 1, hidden, chunk), bf16),
+            pltpu.VMEM((sp, tp, cap, hidden), bf16),
+            pltpu.VMEM((sp, tp, cap, hidden), bf16),
             pltpu.VMEM((sp, cap, width), bf16),
             pltpu.VMEM((sp, tp, cap, width), bf16),
-            pltpu.VMEM((sp, tp, cap, width), bf16),
-            pltpu.VMEM((sp, outer, cap, width), bf16),
-            pltpu.VMEM((sp, outer, cap, width), bf16),
-            pltpu.VMEM((sp, outer, cap, width), bf16),
+            pltpu.VMEM((sp, tp, cap, own_part), bf16),
+            pltpu.VMEM((sp, 2, cap, own_part), bf16),
+            pltpu.VMEM((sp, cap, own_part), bf16),
+            pltpu.VMEM((sp, cap, own_part), bf16),
             pltpu.VMEM((sp, cap, width), bf16),
             pltpu.VMEM((sp, cap, width), bf16),
-            dma, dma((lanes,)), dma((lanes,)), dma((lanes,)), dma((lanes,)),
-            dma((outer, parts)), dma((outer, parts)), dma((outer, parts)), dma((outer, parts)),
-            dma((3,)), dma((sp,)), dma((sp,)),
-            dma((sp, outer)), dma((sp, outer)), dma((sp, outer)), dma((sp, outer)),
-            dma((sp, outer)), dma((sp, outer)), dma((sp, outer)), dma((sp, outer)),
-            dma((sp,)), dma((sp,)),
+            dma((10,)), dma((lanes,)), dma((lanes,)), dma((lanes,)), dma((lanes,)),
+            dma((2, parts)), dma((2, parts)), dma((parts,)), dma((parts,)),
+            dma((chunks, tp - 1)), dma((chunks, tp - 1)), dma((sp, tp - 1)), dma((sp, tp - 1)),
+            dma((sp,)), dma((sp,)), dma((sp,)), dma((sp,)), dma((sp, 2)), dma((sp, 2)),
+            dma((sp, 2)), dma((sp, 2)), dma((sp,)), dma((sp,)), dma((sp,)), dma((sp,)),
         ],
         compiler_params=pltpu.CompilerParams(
             collective_id=0, has_side_effects=True, vmem_limit_bytes=VMEM_BYTES
@@ -443,7 +529,7 @@
     )(
         query_one, key_one, query_two, key_two, value, lambda_head,
         head_gain[None, :], out_weight, residual, norm_gain[None, :],
-        route_expert, route_weight, gate, up, down,
+        route_expert.T, route_weight.T, gate, up, down,
     )
 
 
@@ -460,13 +546,12 @@
     sp, tp = lax.axis_size("sp"), lax.axis_size("tp")
     rows, top_count = route_expert.shape
     return (
-        sp % 2 == 0
-        and tp % 2 == 0
+        sp == 8
+        and tp == 4
         and slots(rows, top_count, sp) % 16 == 0
         and rows % 16 == 0
         and query_one.shape[0] * sp <= 2048
-        and residual.shape[1] % 512 == 0
-        and sp <= 8
+        and residual.shape[1] % 1024 == 0
     )
 
 

time: 111 us -> 103 us (0.928)
  Pallas kernels: 106 us -> 101 us
  local copies, waits for them, and re-layouts: 4.39 us -> 1.67 us
    pallas_call x1, Pallas kernels: 106 us -> 101 us  [layer(): pl.pallas_call(functools.partial(layer_kernel, sp, tp, heads, kv_heads, c...]
    unnamed x3 -> x1, local copies, waits for them, and re-layouts: 4.39 us -> 1.67 us
where the time goes in v1:
time: 103 us
  Pallas kernels  101 us (98%)
  local copies, waits for them, and re-layouts  1.67 us (2%)
    pallas_call x1, Pallas kernels, layer(): pl.pallas_call(functools.partial(layer_kernel, sp, tp, heads, kv_heads, c...  101 us

profile of v1, /device:TPU:0, one launch (start us, length us, event | category | flops | bytes accessed | tf_op | source)
XLA Modules:
  0.0 103.1 jit_solution(14428893686714990799)
XLA Ops:
  0.0 101.4 %layer.1 = bf16[32,4096]{1,0:T(8,128)(2,1)} custom-call(bf16[128,256]{1,0:T(8,128)(2,1)} %q1_hbm.1, bf16[128,128]{1,0:T(8,128)(2,1)} %k1_hbm.1, bf16[128,256]{1,0:T(8,128)(2,1)} %q2_hbm.1, bf16[128,128]{1,0:T(8,128)(2,1)} %k2_hbm.1, bf16[128,256]{1,0:T(8,128)(2,1)} %v_hbm.1, f32[2]{0:T(128)} %lam.1, f32[1,256]{1,0:T(1,128)} %bitcast.11, ...), custom_call_target="tpu_custom_call" | custom-call | tf_op jit(solution)/shard_map/layer/pallas_call | solution.py:485
  101.4 1.7 %copy.17 = bf16[32,4096]{1,0:T(8,128)(2,1)} copy(bf16[32,4096]{1,0:T(8,128)(2,1)} %layer.1) | data formatting | bytes 524288

commit v2 on v1

--- a/solution.py
+++ b/solution.py
@@ -61,10 +61,10 @@
     sp, tp, heads, kv_heads, cap, early,
     q1_hbm, k1_hbm, q2_hbm, k2_hbm, v_hbm, lam, gain, ow_hbm, res_hbm, ngain,
     route_e, route_w, gate_hbm, up_hbm, down_hbm, out,
-    q1, q2, res, kv, ow, att, pbuf, prc, pcs, pry, total, normed, placed, mix,
+    q1, q2, res, kv, ow, att, pbuf, prc, pcs, pry, total, held_rows, placed, tables, mix,
     gate, up, down, moved, hid, hidr, outg, tok, part, rc, cs, ry, fin, ret,
     f_sem, z_send, z_recv, x_send, x_recv, pc_send, pc_recv, py_send, py_recv,
-    d_send, d_recv, h_send, h_recv, a_send, a_recv, y_send, y_recv, c_send, c_recv,
+    t_send, t_recv, r_send, r_recv, d_send, d_recv, h_send, h_recv, a_send, a_recv, y_send, y_recv, c_send, c_recv,
     rc_send, rc_recv, ry_send, ry_recv, ra_send, ra_recv,
 ):
     s = lax.axis_index("sp")
@@ -126,7 +126,7 @@
         preferred_element_type=jnp.float32,
     )
     held = jnp.where(rank == slot, named, 0.0)
-    placed[...] = held.astype(jnp.bfloat16)
+    placed[...] = held.astype(jnp.bfloat16).reshape(sp, cap, rows)
     mix[...] = share * held
 
     sends = []
@@ -135,11 +135,16 @@
         copy.start()
         sends.append(copy)
 
-    def along(block, to, d):
-        return remote(kv.at[block], kv.at[block], z_send.at[d], z_recv.at[d], to, t)
-
-    def across(block, d):
-        return remote(kv.at[block], kv.at[block], x_send.at[d], x_recv.at[d], px, t)
+    pieces = z_send.shape[1]
+    span = local // pieces
+
+    def along(block, to, d, i):
+        part_of = kv.at[block, i * span:(i + 1) * span]
+        return remote(part_of, part_of, z_send.at[d, i], z_recv.at[d, i], to, t)
+
+    def across(block, d, i):
+        part_of = kv.at[block, i * span:(i + 1) * span]
+        return remote(part_of, part_of, x_send.at[d, i], x_recv.at[d, i], px, t)
 
     for copy in fetches[:3]:
         copy.wait()
@@ -147,11 +152,13 @@
     for d in (2, 1):
         @pl.when(z + d < lanes)
         def _():
-            along(s, s + 2 * d, d).start()
+            for i in range(pieces):
+                along(s, s + 2 * d, d, i).start()
 
     @pl.when(x == 0)
     def _():
-        across(s, 0).start()
+        for i in range(pieces):
+            across(s, 0, i).start()
 
     def lend(n, r):
         to = flipped(t, r)
@@ -165,6 +172,16 @@
         return remote(
             moved.at[n, 1], moved.at[n, 2], d_send.at[n, 2], d_recv.at[n, 2], s, core
         )
+
+    def table(j):
+        there = flipped(s, 2 * j)
+        pair_of = pl.ds(2 * lax.div(there, 2), 2)
+        return remote(
+            placed.at[pair_of], tables.at[j], t_send.at[j], t_recv.at[j], there, t
+        )
+
+    for j in range(1, lanes):
+        begin(table(j))
 
     fetches[3].wait()
     for n in range(early):
@@ -176,16 +193,19 @@
         @pl.when(z == level)
         def _():
             for d in order:
-                along(s - 2 * d, s, d).wait_recv()
-                if level + d == 4 and d == 2:
-                    along(s - 2 * d, s + 2, 3).start()
-                across(s - 2 * d, d).start()
+                for i in range(pieces):
+                    along(s - 2 * d, s, d, i).wait_recv()
+                    if level + d == 4 and d == 2:
+                        along(s - 2 * d, s + 2, 3, i).start()
+                    across(s - 2 * d, d, i).start()
             for d in order:
-                across(px - 2 * d, d).wait_recv()
+                for i in range(pieces):
+                    across(px - 2 * d, d, i).wait_recv()
 
     @pl.when(x == 1)
     def _():
-        across(px, 0).wait_recv()
+        for i in range(pieces):
+            across(px, 0, i).wait_recv()
 
     for copy in fetches[4:6]:
         copy.wait()
@@ -267,19 +287,53 @@
         summed += jnp.sum(piece, axis=-1, keepdims=True)
     centered = total[...] - summed / width
     variance = jnp.mean(centered * centered, axis=-1, keepdims=True)
-    normed[...] = (centered * lax.rsqrt(variance + 1e-05) * ngain[...]).astype(jnp.bfloat16)
+    held_rows[0] = (centered * lax.rsqrt(variance + 1e-05) * ngain[...]).astype(jnp.bfloat16)
 
     tile = math.gcd(width, 1024)
 
-    @pl.loop(0, width // tile)
-    def _(n):
-        columns = pl.ds(pl.multiple_of(n * tile, tile), tile)
-        piece = jnp.dot(placed[...], normed[:, columns], preferred_element_type=jnp.float32)
-        outg[:, :, columns] = piece.astype(jnp.bfloat16).reshape(sp, cap, tile)
-
-    def arrive(k):
-        there = flipped(s, k)
-        return remote(outg.at[there], tok.at[k, t], a_send.at[k], a_recv.at[k], there, t)
+    inner = (z > 0) & (z < lanes - 1)
+
+    def to_row(j):
+        return remote(
+            held_rows.at[0], held_rows.at[j], r_send.at[j], r_recv.at[j], flipped(s, 2 * j), t
+        )
+
+    def pass_row():
+        return remote(
+            held_rows.at[2], held_rows.at[3], r_send.at[0], r_recv.at[3], flipped(s, 2), t
+        )
+
+    begin(to_row(1))
+    begin(to_row(2))
+
+    @pl.when(inner)
+    def _():
+        to_row(3).start()
+
+    def arrive(j):
+        k = 2 * j + 1
+        return remote(outg.at[j], tok.at[k, t], a_send.at[k], a_recv.at[k], px, t)
+
+    def select(j):
+        if j:
+            to_row(j).wait_recv()
+        if j == 2:
+            @pl.when(inner)
+            def _():
+                pass_row().start()
+        if j:
+            table(j).wait_recv()
+            mine, other = tables[j, x], tables[j, 1 - x]
+        else:
+            mine, other = placed[s], placed[px]
+        both = jnp.concatenate([mine, other], axis=0)
+        for n in range(width // tile):
+            columns = slice(n * tile, (n + 1) * tile)
+            piece = jnp.dot(both, held_rows[j, :, columns], preferred_element_type=jnp.float32)
+            piece = piece.astype(jnp.bfloat16)
+            tok[2 * j, t, :, columns] = piece[:cap]
+            outg[j, :, columns] = piece[cap:]
+        begin(arrive(j))
 
     def plane(k):
         return remote(
@@ -314,20 +368,20 @@
         remote(tok.at[k, group], tok.at[k, group], send, recv, s, core).wait_recv()
 
     order = step_order(sp)
-    for k in order:
-        if k:
-            begin(arrive(k))
-    tok[0, t] = outg[s]
 
     def spread(k):
-        if k:
+        if k % 2:
             landed_tok(k, t, a_send.at[k], a_recv.at[k])
+        else:
+            select(k // 2)
         begin(plane(k))
         begin(pair(k, 0))
 
-    def collect(k):
+    def relay(k):
         landed_tok(k, plane_peer, y_send.at[k], y_recv.at[k])
         begin(pair(k, 1))
+
+    def collect(k):
         landed_tok(k, core, c_send.at[k, 0], c_recv.at[k, 0])
         landed_tok(k, corner, c_send.at[k, 1], c_recv.at[k, 1])
 
@@ -386,29 +440,33 @@
             else:
                 ret[s] = fin[k]
 
-    lead = 2
-    for k in order[:lead]:
+    lead, lag = 3, 1
+    for k in [0] + order[:lead - 1]:
         spread(k)
+    relay(order[0])
+    for n in range(chunks):
+        lend(n, 2).wait_recv()
+        begin(relend(n))
+    for copy in fetches[8:10]:
+        copy.wait()
     for i, k in enumerate(order):
+        collect(k)
+        compute(k)
         if i == 0:
-            for n in range(chunks):
-                lend(n, 2).wait_recv()
-                begin(relend(n))
-        collect(k)
-        if i == 0:
-            for copy in fetches[8:10]:
-                copy.wait()
-        compute(k)
-        if i == 1:
+            relay(0)
+        if i + 1 < len(order) - 1:
+            relay(order[i + 1])
+        reduce_pair(k)
+        if i + lead < len(order):
+            spread(order[i + lead - 1])
+        if i == lag:
             for n in range(chunks):
                 lend(n, 1).wait_recv()
                 relend(n).wait_recv()
-        if i % 2 and i > 1:
-            finish_steps(order[i - 3:i - 1])
-        reduce_pair(k)
-        if i + lead < len(order):
-            spread(order[i + lead])
-    finish_steps(order[-2:])
+        if i >= lag:
+            finish_steps([order[i - lag]])
+    for k in order[len(order) - lag:]:
+        finish_steps([k])
     for k in range(1, sp):
         there = flipped(s, k)
         remote(ret.at[there], ret.at[there], ra_send.at[k], ra_recv.at[k], s, core).wait_recv()
@@ -433,33 +491,40 @@
         returned = ret[:, :, columns].reshape(sp * cap, tile)
         combined = jnp.dot(mix_high, returned, preferred_element_type=jnp.float32)
         combined += jnp.dot(mix_low, returned, preferred_element_type=jnp.float32)
-        out[:, columns] = (normed[:, columns].astype(jnp.float32) + combined).astype(
+        out[:, columns] = (held_rows[0, :, columns].astype(jnp.float32) + combined).astype(
             jnp.bfloat16
         )
 
     for copy in sends:
         copy.wait_send()
-    for d in (2, 1):
-        @pl.when(z + d < lanes)
+
+    @pl.when(inner)
+    def _():
+        to_row(3).wait_send()
+        pass_row().wait_send()
+
+    for i in range(pieces):
+        for d in (2, 1):
+            @pl.when(z + d < lanes)
+            def _():
+                along(s, s + 2 * d, d, i).wait_send()
+
+        @pl.when(x == 0)
         def _():
-            along(s, s + 2 * d, d).wait_send()
-
-    @pl.when(x == 0)
-    def _():
-        across(s, 0).wait_send()
-
-    for level, order_of in ((1, (1,)), (2, (2, 1)), (3, (1, 2, 3))):
-        @pl.when(z == level)
-        def _():
-            for d in order_of:
-                if level + d == 4 and d == 2:
-                    along(s - 2 * d, s + 2, 3).wait_send()
-                across(s - 2 * d, d).wait_send()
+            across(s, 0, i).wait_send()
+
+        for level, order_of in ((1, (1,)), (2, (2, 1)), (3, (1, 2, 3))):
+            @pl.when(z == level)
+            def _():
+                for d in order_of:
+                    if level + d == 4 and d == 2:
+                        along(s - 2 * d, s + 2, 3, i).wait_send()
+                    across(s - 2 * d, d, i).wait_send()
 
 
 def step_order(sp):
-    far = [k for half in (3, 2) for k in (2 * half, 2 * half + 1)]
-    return [0, 1, 2] + far + [3]
+    far = [k for half in range(2, sp // 2) for k in (2 * half, 2 * half + 1)]
+    return [1, 2] + far + [3, 0]
 
 
 def layer(
@@ -499,8 +564,9 @@
             pltpu.VMEM((parts, rows, width // parts), bf16),
             pltpu.VMEM((parts, rows, width // parts), bf16),
             pltpu.VMEM((rows, width), jnp.float32),
-            pltpu.VMEM((rows, width), bf16),
-            pltpu.VMEM((sp * cap, rows), bf16),
+            pltpu.VMEM((lanes, rows, width), bf16),
+            pltpu.VMEM((sp, cap, rows), bf16),
+            pltpu.VMEM((lanes, 2, cap, rows), bf16),
             pltpu.VMEM((sp * cap, rows), jnp.float32),
             pltpu.VMEM((width, hidden), bf16),
             pltpu.VMEM((width, hidden), bf16),
@@ -508,7 +574,7 @@
             pltpu.VMEM((chunks, tp - 1, hidden, chunk), bf16),
             pltpu.VMEM((sp, tp, cap, hidden), bf16),
             pltpu.VMEM((sp, tp, cap, hidden), bf16),
-            pltpu.VMEM((sp, cap, width), bf16),
+            pltpu.VMEM((lanes, cap, width), bf16),
             pltpu.VMEM((sp, tp, cap, width), bf16),
             pltpu.VMEM((sp, tp, cap, own_part), bf16),
             pltpu.VMEM((sp, 2, cap, own_part), bf16),
@@ -516,8 +582,9 @@
             pltpu.VMEM((sp, cap, own_part), bf16),
             pltpu.VMEM((sp, cap, width), bf16),
             pltpu.VMEM((sp, cap, width), bf16),
-            dma((10,)), dma((lanes,)), dma((lanes,)), dma((lanes,)), dma((lanes,)),
+            dma((10,)), dma((lanes, 2)), dma((lanes, 2)), dma((lanes, 2)), dma((lanes, 2)),
             dma((2, parts)), dma((2, parts)), dma((parts,)), dma((parts,)),
+            dma((lanes,)), dma((lanes,)), dma((lanes,)), dma((lanes,)),
             dma((chunks, tp - 1)), dma((chunks, tp - 1)), dma((sp, tp - 1)), dma((sp, tp - 1)),
             dma((sp,)), dma((sp,)), dma((sp,)), dma((sp,)), dma((sp, 2)), dma((sp, 2)),
             dma((sp, 2)), dma((sp, 2)), dma((sp,)), dma((sp,)), dma((sp,)), dma((sp,)),

time: 103 us -> 92.6 us (0.90)
  Pallas kernels: 101 us -> 90.4 us
    pallas_call x1, Pallas kernels: 101 us -> 90.4 us  [layer(): pl.pallas_call(functools.partial(layer_kernel, sp, tp, heads, kv_heads, c...]
where the time goes in v2:
time: 92.6 us; the launch traced here: 92.1 us
  Pallas kernels  90.4 us (98%)
  local copies, waits for them, and re-layouts  1.67 us (2%)
    pallas_call x1, Pallas kernels, layer(): pl.pallas_call(functools.partial(layer_kernel, sp, tp, heads, kv_heads, c...  90.4 us

profile of v2, /device:TPU:0, one launch (start us, length us, event | category | flops | bytes accessed | tf_op | source)
XLA Modules:
  0.0 92.1 jit_solution(5601249322612305156)
XLA Ops:
  0.0 90.4 %layer.1 = bf16[32,4096]{1,0:T(8,128)(2,1)} custom-call(bf16[128,256]{1,0:T(8,128)(2,1)} %q1_hbm.1, bf16[128,128]{1,0:T(8,128)(2,1)} %k1_hbm.1, bf16[128,256]{1,0:T(8,128)(2,1)} %q2_hbm.1, bf16[128,128]{1,0:T(8,128)(2,1)} %k2_hbm.1, bf16[128,256]{1,0:T(8,128)(2,1)} %v_hbm.1, f32[2]{0:T(128)} %lam.1, f32[1,256]{1,0:T(1,128)} %bitcast.11, ...), custom_call_target="tpu_custom_call" | custom-call | tf_op jit(solution)/shard_map/layer/pallas_call | solution.py:550
  90.4 1.7 %copy.17 = bf16[32,4096]{1,0:T(8,128)(2,1)} copy(bf16[32,4096]{1,0:T(8,128)(2,1)} %layer.1) | data formatting | bytes 524288

commit v3 on v2

--- a/solution.py
+++ b/solution.py
@@ -11,6 +11,11 @@
 HEAD = 128
 VMEM_BYTES = 58 * 1024 * 1024
 CHUNKS, EARLY = 4, 3
+PLAN = (
+    "s0 s1 l0 s2", "r1 c1 s4 s3", "r2 w0 p1 c2", "s5 r4 f1 p2",
+    "c4 s6 r5 f2", "p4 c5 s7 r6", "f4 p5 c6 r7", "f5 p6 r3 c7",
+    "r0 f6 p7 c3", "f7 p3 c0 f3", "p0 f0",
+)
 
 
 def map_step(carried, query_rows, key_block, value_block, allowed):
@@ -65,7 +70,7 @@
     gate, up, down, moved, hid, hidr, outg, tok, part, rc, cs, ry, fin, ret,
     f_sem, z_send, z_recv, x_send, x_recv, pc_send, pc_recv, py_send, py_recv,
     t_send, t_recv, r_send, r_recv, d_send, d_recv, h_send, h_recv, a_send, a_recv, y_send, y_recv, c_send, c_recv,
-    rc_send, rc_recv, ry_send, ry_recv, ra_send, ra_recv,
+    rc_send, rc_recv, ry_send, ry_recv, ra_send, ra_recv, result, o_sem,
 ):
     s = lax.axis_index("sp")
     t = lax.axis_index("tp")
@@ -367,8 +372,6 @@
     def landed_tok(k, group, send, recv):
         remote(tok.at[k, group], tok.at[k, group], send, recv, s, core).wait_recv()
 
-    order = step_order(sp)
-
     def spread(k):
         if k % 2:
             landed_tok(k, t, a_send.at[k], a_recv.at[k])
@@ -440,33 +443,25 @@
             else:
                 ret[s] = fin[k]
 
-    lead, lag = 3, 1
-    for k in [0] + order[:lead - 1]:
-        spread(k)
-    relay(order[0])
-    for n in range(chunks):
-        lend(n, 2).wait_recv()
-        begin(relend(n))
-    for copy in fetches[8:10]:
-        copy.wait()
-    for i, k in enumerate(order):
-        collect(k)
-        compute(k)
-        if i == 0:
-            relay(0)
-        if i + 1 < len(order) - 1:
-            relay(order[i + 1])
-        reduce_pair(k)
-        if i + lead < len(order):
-            spread(order[i + lead - 1])
-        if i == lag:
-            for n in range(chunks):
-                lend(n, 1).wait_recv()
-                relend(n).wait_recv()
-        if i >= lag:
-            finish_steps([order[i - lag]])
-    for k in order[len(order) - lag:]:
-        finish_steps([k])
+    def begin_lent(_):
+        for n in range(chunks):
+            lend(n, 2).wait_recv()
+            begin(relend(n))
+        for copy in fetches[8:10]:
+            copy.wait()
+
+    def wait_lent(_):
+        for n in range(chunks):
+            lend(n, 1).wait_recv()
+            relend(n).wait_recv()
+
+    actions = {
+        "s": [spread], "r": [relay], "c": [collect, compute], "p": [reduce_pair],
+        "f": [lambda k: finish_steps([k])], "l": [begin_lent], "w": [wait_lent],
+    }
+    for action in " ".join(PLAN).split():
+        for part_of in actions[action[0]]:
+            part_of(int(action[1]))
     for k in range(1, sp):
         there = flipped(s, k)
         remote(ret.at[there], ret.at[there], ra_send.at[k], ra_recv.at[k], s, core).wait_recv()
@@ -485,15 +480,19 @@
     mix_low = turned((mix[...] - high.astype(jnp.float32)).astype(jnp.bfloat16))
     mix_high = turned(high)
 
-    @pl.loop(0, width // tile)
-    def _(n):
-        columns = pl.ds(pl.multiple_of(n * tile, tile), tile)
+    leaving = []
+    for n in range(width // tile):
+        columns = slice(n * tile, (n + 1) * tile)
         returned = ret[:, :, columns].reshape(sp * cap, tile)
         combined = jnp.dot(mix_high, returned, preferred_element_type=jnp.float32)
         combined += jnp.dot(mix_low, returned, preferred_element_type=jnp.float32)
-        out[:, columns] = (held_rows[0, :, columns].astype(jnp.float32) + combined).astype(
+        result[:, columns] = (held_rows[0, :, columns].astype(jnp.float32) + combined).astype(
             jnp.bfloat16
         )
+        leaving.append(
+            pltpu.make_async_copy(result.at[:, columns], out.at[:, columns], o_sem.at[n])
+        )
+        leaving[-1].start()
 
     for copy in sends:
         copy.wait_send()
@@ -521,10 +520,8 @@
                         along(s - 2 * d, s + 2, 3, i).wait_send()
                     across(s - 2 * d, d, i).wait_send()
 
-
-def step_order(sp):
-    far = [k for half in range(2, sp // 2) for k in (2 * half, 2 * half + 1)]
-    return [1, 2] + far + [3, 0]
+    for copy in leaving:
+        copy.wait()
 
 
 def layer(
@@ -551,7 +548,7 @@
         functools.partial(layer_kernel, sp, tp, heads, kv_heads, cap, early),
         out_shape=jax.ShapeDtypeStruct((rows, width), bf16),
         in_specs=[hbm] * 5 + [smem, vmem, hbm, hbm] + [vmem] * 3 + [hbm] * 3,
-        out_specs=vmem,
+        out_specs=hbm,
         scratch_shapes=[
             pltpu.VMEM(query_one.shape, bf16),
             pltpu.VMEM(query_two.shape, bf16),
@@ -582,12 +579,13 @@
             pltpu.VMEM((sp, cap, own_part), bf16),
             pltpu.VMEM((sp, cap, width), bf16),
             pltpu.VMEM((sp, cap, width), bf16),
-            dma((10,)), dma((lanes, 2)), dma((lanes, 2)), dma((lanes, 2)), dma((lanes, 2)),
+            dma((10,)), dma((lanes, 4)), dma((lanes, 4)), dma((lanes, 4)), dma((lanes, 4)),
             dma((2, parts)), dma((2, parts)), dma((parts,)), dma((parts,)),
             dma((lanes,)), dma((lanes,)), dma((lanes,)), dma((lanes,)),
             dma((chunks, tp - 1)), dma((chunks, tp - 1)), dma((sp, tp - 1)), dma((sp, tp - 1)),
             dma((sp,)), dma((sp,)), dma((sp,)), dma((sp,)), dma((sp, 2)), dma((sp, 2)),
             dma((sp, 2)), dma((sp, 2)), dma((sp,)), dma((sp,)), dma((sp,)), dma((sp,)),
+            pltpu.VMEM((rows, width), bf16), dma((width // math.gcd(width, 1024),)),
         ],
         compiler_params=pltpu.CompilerParams(
             collective_id=0, has_side_effects=True, vmem_limit_bytes=VMEM_BYTES

time: 92.6 us -> 91.3 us (0.986)
  Pallas kernels: 90.4 us -> 88.5 us
    pallas_call x1, Pallas kernels: 90.4 us -> 88.5 us  [layer(): pl.pallas_call(functools.partial(layer_kernel, sp, tp, heads, kv_heads, c...]
where the time goes in v3:
time: 91.3 us; the launch traced here: 90.2 us
  Pallas kernels  88.5 us (97%)
  local copies, waits for them, and re-layouts  1.67 us (2%)
    pallas_call x1, Pallas kernels, layer(): pl.pallas_call(functools.partial(layer_kernel, sp, tp, heads, kv_heads, c...  88.5 us

profile of v3, /device:TPU:0, one launch (start us, length us, event | category | flops | bytes accessed | tf_op | source)
XLA Modules:
  0.0 90.2 jit_solution(221201905026359909)
XLA Ops:
  0.0 88.5 %layer.1 = bf16[32,4096]{1,0:T(8,128)(2,1)} custom-call(bf16[128,256]{1,0:T(8,128)(2,1)} %q1_hbm.1, bf16[128,128]{1,0:T(8,128)(2,1)} %k1_hbm.1, bf16[128,256]{1,0:T(8,128)(2,1)} %q2_hbm.1, bf16[128,128]{1,0:T(8,128)(2,1)} %k2_hbm.1, bf16[128,256]{1,0:T(8,128)(2,1)} %v_hbm.1, f32[2]{0:T(128)} %lam.1, f32[1,256]{1,0:T(1,128)} %bitcast.11, ...), custom_call_target="tpu_custom_call" | custom-call | tf_op jit(solution)/shard_map/layer/pallas_call | solution.py:547
  88.5 1.7 %copy.17 = bf16[32,4096]{1,0:T(8,128)(2,1)} copy(bf16[32,4096]{1,0:T(8,128)(2,1)} %layer.1) | data formatting | bytes 524288

commit v4 on v3

--- a/solution.py
+++ b/solution.py
@@ -12,9 +12,10 @@
 VMEM_BYTES = 58 * 1024 * 1024
 CHUNKS, EARLY = 4, 3
 PLAN = (
-    "s0 s1 l0 s2", "r1 c1 s4 s3", "r2 w0 p1 c2", "s5 r4 f1 p2",
-    "c4 s6 r5 f2", "p4 c5 s7 r6", "f4 p5 c6 r7", "f5 p6 r3 c7",
-    "r0 f6 p7 c3", "f7 p3 c0 f3", "p0 f0",
+    "s0 s1 l0 s2", "r1 c1 s4 s3", "r2 w0 p1 c2", "s5 h1 r4 p2",
+    "f1 c4 h2 s6", "r5 p4 f2 c5", "h4 s7 r6 p5", "f4 c6 h5 r7",
+    "p6 f5 r3 c7", "h6 r0 p7 f6", "c3 h7 p3 f7", "c0 h3 p0 f3",
+    "h0 f0",
 )
 
 
@@ -366,8 +367,14 @@
             hid.at[k, to], hidr.at[k, r], h_send.at[k, r - 1], h_recv.at[k, r - 1], s, to
         )
 
-    def back(k):
-        return remote(fin.at[k], ret.at[s], ra_send.at[k], ra_recv.at[k], flipped(s, k), t)
+    halves = (slice(0, shared), slice(shared, width))
+
+    def back(k, half):
+        columns = halves[half]
+        return remote(
+            fin.at[k, :, columns], ret.at[s, :, columns],
+            ra_send.at[k, half], ra_recv.at[k, half], flipped(s, k), t,
+        )
 
     def landed_tok(k, group, send, recv):
         remote(tok.at[k, group], tok.at[k, group], send, recv, s, core).wait_recv()
@@ -419,29 +426,30 @@
         ).astype(jnp.bfloat16)
         begin(back_plane(k))
 
-    def finish_steps(ks):
-        for k in ks:
-            for r in range(1, tp):
-                pass_hidden(k, r).wait_recv()
-        lefts = [jnp.concatenate([hidr[k, r] for k in ks], axis=0) for r in range(tp)]
+    def finish_shared(k):
+        for r in range(1, tp):
+            pass_hidden(k, r).wait_recv()
         for n in range(chunks):
             columns = slice(n * chunk, (n + 1) * chunk)
-            piece = jnp.dot(lefts[0], down[:, columns], preferred_element_type=jnp.float32)
+            piece = jnp.dot(hidr[k, 0], down[:, columns], preferred_element_type=jnp.float32)
             for r in range(1, tp):
-                piece += jnp.dot(lefts[r], moved[n, r - 1], preferred_element_type=jnp.float32)
-            piece = piece.astype(jnp.bfloat16)
-            for i, k in enumerate(ks):
-                fin[k, :, columns] = piece[i * cap:(i + 1) * cap]
-        for k in ks:
-            back_pair(k, 0).wait_recv()
-            whole = part[k, t].astype(jnp.float32) + rc[k, 0].astype(jnp.float32)
-            back_plane(k).wait_recv()
-            whole = whole + ry[k].astype(jnp.float32)
-            fin[k, :, shared:] = whole.astype(jnp.bfloat16)
-            if k:
-                begin(back(k))
-            else:
-                ret[s] = fin[k]
+                piece += jnp.dot(hidr[k, r], moved[n, r - 1], preferred_element_type=jnp.float32)
+            fin[k, :, columns] = piece.astype(jnp.bfloat16)
+        if k:
+            begin(back(k, 0))
+        else:
+            ret[s, :, :shared] = fin[k, :, :shared]
+
+    def finish_own(k):
+        back_pair(k, 0).wait_recv()
+        whole = part[k, t].astype(jnp.float32) + rc[k, 0].astype(jnp.float32)
+        back_plane(k).wait_recv()
+        whole = whole + ry[k].astype(jnp.float32)
+        fin[k, :, shared:] = whole.astype(jnp.bfloat16)
+        if k:
+            begin(back(k, 1))
+        else:
+            ret[s, :, shared:] = fin[k, :, shared:]
 
     def begin_lent(_):
         for n in range(chunks):
@@ -457,14 +465,16 @@
 
     actions = {
         "s": [spread], "r": [relay], "c": [collect, compute], "p": [reduce_pair],
-        "f": [lambda k: finish_steps([k])], "l": [begin_lent], "w": [wait_lent],
+        "f": [finish_own], "h": [finish_shared], "l": [begin_lent], "w": [wait_lent],
     }
     for action in " ".join(PLAN).split():
         for part_of in actions[action[0]]:
             part_of(int(action[1]))
     for k in range(1, sp):
         there = flipped(s, k)
-        remote(ret.at[there], ret.at[there], ra_send.at[k], ra_recv.at[k], s, core).wait_recv()
+        for half, columns in enumerate(halves):
+            landed = ret.at[there, :, columns]
+            remote(landed, landed, ra_send.at[k, half], ra_recv.at[k, half], s, core).wait_recv()
 
     unit = lax.broadcasted_iota(jnp.int32, (sp * cap, sp * cap), 0) == lax.broadcasted_iota(
         jnp.int32, (sp * cap, sp * cap), 1
@@ -584,7 +594,7 @@
             dma((lanes,)), dma((lanes,)), dma((lanes,)), dma((lanes,)),
             dma((chunks, tp - 1)), dma((chunks, tp - 1)), dma((sp, tp - 1)), dma((sp, tp - 1)),
             dma((sp,)), dma((sp,)), dma((sp,)), dma((sp,)), dma((sp, 2)), dma((sp, 2)),
-            dma((sp, 2)), dma((sp, 2)), dma((sp,)), dma((sp,)), dma((sp,)), dma((sp,)),
+            dma((sp, 2)), dma((sp, 2)), dma((sp,)), dma((sp,)), dma((sp, 2)), dma((sp, 2)),
             pltpu.VMEM((rows, width), bf16), dma((width // math.gcd(width, 1024),)),
         ],
         compiler_params=pltpu.CompilerParams(

time: 91.3 us -> 89.8 us (0.984)
    pallas_call x1, Pallas kernels: 88.5 us -> 87.6 us  [layer(): pl.pallas_call(functools.partial(layer_kernel, sp, tp, heads, kv_heads, c...]
where the time goes in v4:
time: 89.8 us; the launch traced here: 89.2 us
  Pallas kernels  87.6 us (98%)
  local copies, waits for them, and re-layouts  1.67 us (2%)
    pallas_call x1, Pallas kernels, layer(): pl.pallas_call(functools.partial(layer_kernel, sp, tp, heads, kv_heads, c...  87.6 us

profile of v4, /device:TPU:0, one launch (start us, length us, event | category | flops | bytes accessed | tf_op | source)
XLA Modules:
  0.0 89.2 jit_solution(9287690775551631154)
XLA Ops:
  0.0 87.6 %layer.1 = bf16[32,4096]{1,0:T(8,128)(2,1)} custom-call(bf16[128,256]{1,0:T(8,128)(2,1)} %q1_hbm.1, bf16[128,128]{1,0:T(8,128)(2,1)} %k1_hbm.1, bf16[128,256]{1,0:T(8,128)(2,1)} %q2_hbm.1, bf16[128,128]{1,0:T(8,128)(2,1)} %k2_hbm.1, bf16[128,256]{1,0:T(8,128)(2,1)} %v_hbm.1, f32[2]{0:T(128)} %lam.1, f32[1,256]{1,0:T(1,128)} %bitcast.11, ...), custom_call_target="tpu_custom_call" | custom-call | tf_op jit(solution)/shard_map/layer/pallas_call | solution.py:557
  87.6 1.7 %copy.17 = bf16[32,4096]{1,0:T(8,128)(2,1)} copy(bf16[32,4096]{1,0:T(8,128)(2,1)} %layer.1) | data formatting | bytes 524288

commit v5 on v4

--- a/solution.py
+++ b/solution.py
@@ -13,7 +13,7 @@
 CHUNKS, EARLY = 4, 3
 PLAN = (
     "s0 s1 l0 s2", "r1 c1 s4 s3", "r2 w0 p1 c2", "s5 h1 r4 p2",
-    "f1 c4 h2 s6", "r5 p4 f2 c5", "h4 s7 r6 p5", "f4 c6 h5 r7",
+    "c4 f1 h2 s6", "r5 p4 f2 c5", "h4 s7 r6 p5", "f4 c6 h5 r7",
     "p6 f5 r3 c7", "h6 r0 p7 f6", "c3 h7 p3 f7", "c0 h3 p0 f3",
     "h0 f0",
 )

time: 89.8 us -> 89.9 us (level)
  no operation moved by 1% of the time
where the time goes in v5:
time: 89.9 us; the launch traced here: 89.2 us
  Pallas kernels  87.5 us (97%)
  local copies, waits for them, and re-layouts  1.67 us (2%)
    pallas_call x1, Pallas kernels, layer(): pl.pallas_call(functools.partial(layer_kernel, sp, tp, heads, kv_heads, c...  87.5 us

profile of v5, /device:TPU:0, one launch (start us, length us, event | category | flops | bytes accessed | tf_op | source)
XLA Modules:
  0.0 89.2 jit_solution(6575764778819721992)
XLA Ops:
  0.0 87.5 %layer.1 = bf16[32,4096]{1,0:T(8,128)(2,1)} custom-call(bf16[128,256]{1,0:T(8,128)(2,1)} %q1_hbm.1, bf16[128,128]{1,0:T(8,128)(2,1)} %k1_hbm.1, bf16[128,256]{1,0:T(8,128)(2,1)} %q2_hbm.1, bf16[128,128]{1,0:T(8,128)(2,1)} %k2_hbm.1, bf16[128,256]{1,0:T(8,128)(2,1)} %v_hbm.1, f32[2]{0:T(128)} %lam.1, f32[1,256]{1,0:T(1,128)} %bitcast.11, ...), custom_call_target="tpu_custom_call" | custom-call | tf_op jit(solution)/shard_map/layer/pallas_call | solution.py:557
  87.5 1.7 %copy.17 = bf16[32,4096]{1,0:T(8,128)(2,1)} copy(bf16[32,4096]{1,0:T(8,128)(2,1)} %layer.1) | data formatting | bytes 524288
